TPU v7x, 32 devices: a whole 2x2x4 slice. The times are simulated.
32 devices in a mesh: sp: 16 (over z, y, core), tp: 2 (over x).
Axes of the slice: x: 2, y: 2, z: 4, core: 2. Of those that a mesh axis runs over, the one named last changes fastest.
Arguments:
- tokens: bfloat16 [2048, 2048], P(('sp', 'tp')), may hold values from -16 to 16
- w_query: bfloat16 [2048, 1024], P(None, 'tp'), may hold values from -0.110485435 to 0.110485435
- w_key: bfloat16 [2048, 256], P(None, 'tp'), may hold values from -0.15467961 to 0.15467961
- w_value: bfloat16 [2048, 256], P(None, 'tp'), may hold values from -0.125 to 0.125
- cum_gate: float32 [2048, 16], P('sp', 'tp'), may hold values from -371 to 0, as said below
- w_out: bfloat16 [1024, 2048], replicated, may hold values from -0.1875 to 0.1875
Outputs:
- mixed: bfloat16 [2048, 2048], P(('sp', 'tp'))
Inputs may be any that keep to these rules, and one draw needn't show every extreme that they name: `cum_gate`: each head's column does not rise along the positions.
All inputs are finite; a program needn't handle non-finite values.
Results may differ from a plain program's by a relative error of at most 0.012.
Values may be sent and summed in bfloat16 or wider, within the bound.
A program may use at most 64 MiB of HBM per device.

v0:
```python
import math
import jax
import jax.numpy as jnp
from jax import lax
from jax.sharding import PartitionSpec as P

HEAD_DIM = 64
NEG_FILL = -1e30


def shards(tokens, w_query, w_key, w_value, cum_gate, w_out):
    query_cols = w_query.shape[1]
    pair_cols = w_key.shape[1]
    local_heads = query_cols // HEAD_DIM
    local_kv = pair_cols // HEAD_DIM
    group = local_heads // local_kv
    stacked = jnp.concatenate((w_query, w_key, w_value), axis=1)
    joined = jnp.dot(
        lax.all_gather(tokens, "tp", axis=0, tiled=True),
        stacked,
        preferred_element_type=jnp.float32,
    ).astype(jnp.bfloat16)
    row_count = joined.shape[0]
    queries = joined[:, :query_cols].reshape(row_count, local_kv, group, HEAD_DIM)
    keys = joined[:, query_cols : query_cols + pair_cols]
    values = joined[:, query_cols + pair_cols :]
    gate_query = cum_gate.reshape(row_count, local_kv, group)
    gate_every = lax.all_gather(cum_gate, "sp", axis=0, tiled=True)
    keys_every, values_every = (
        lax.all_gather(keys, "sp", axis=0, tiled=True),
        lax.all_gather(values, "sp", axis=0, tiled=True),
    )
    length = keys_every.shape[0]
    width = math.gcd(length, 2048)
    position_shift = lax.axis_index("sp") * row_count
    query_pos = position_shift + jnp.arange(row_count, dtype=jnp.int32)
    last_pos = position_shift + row_count - 1
    scale = HEAD_DIM ** (-0.5)

    def add_block(index, state):
        run_max, run_total, run_acc = state
        block_start = index * width
        key_block = lax.dynamic_slice_in_dim(keys_every, block_start, width, 0)
        value_block = lax.dynamic_slice_in_dim(values_every, block_start, width, 0)
        gate_block = lax.dynamic_slice_in_dim(gate_every, block_start, width, 0)
        gate_key = gate_block.reshape(width, local_kv, group).transpose(1, 2, 0)
        scores = jnp.einsum(
            "tkgd,rkd->tkgr",
            queries,
            key_block.reshape(width, local_kv, HEAD_DIM),
            preferred_element_type=jnp.float32,
        )
        scores = scores * scale + gate_query[..., None] - gate_key[None]
        key_pos = block_start + jnp.arange(width, dtype=jnp.int32)
        allowed = (key_pos[None, :] <= query_pos[:, None])[:, None, None, :]
        scores = jnp.where(allowed, scores, NEG_FILL)
        new_max = jnp.maximum(run_max, jnp.max(scores, axis=-1))
        weights = jnp.where(allowed, jnp.exp(scores - new_max[..., None]), 0.0)
        factor = jnp.exp(run_max - new_max)
        new_total = run_total * factor + jnp.sum(weights, axis=-1)
        gained = jnp.einsum(
            "tkgr,rkd->tkgd",
            weights.astype(jnp.bfloat16),
            value_block.reshape(width, local_kv, HEAD_DIM),
            preferred_element_type=jnp.float32,
        )
        return (new_max, new_total, run_acc * factor[..., None] + gained)

    initial = (
        jnp.full((row_count, local_kv, group), NEG_FILL, jnp.float32),
        jnp.zeros((row_count, local_kv, group), jnp.float32),
        jnp.zeros((row_count, local_kv, group, HEAD_DIM), jnp.float32),
    )
    run_max, run_total, run_acc = lax.fori_loop(0, last_pos // width + 1, add_block, initial)
    attended = (run_acc / run_total[..., None]).astype(jnp.bfloat16).reshape(row_count, query_cols)
    regrouped = lax.all_to_all(attended, "tp", split_axis=0, concat_axis=1, tiled=True)
    return jnp.dot(regrouped, w_out, preferred_element_type=jnp.float32).astype(jnp.bfloat16)


def solution(mesh):
    placed = (
        P(("sp", "tp"), None),
        P(None, "tp"),
        P(None, "tp"),
        P(None, "tp"),
        P("sp", "tp"),
        P(),
    )
    return jax.shard_map(
        shards, mesh=mesh, in_specs=placed, out_specs=P(("sp", "tp"), None), check_vma=False
    )
```

profile of v0, /device:TPU:0, one launch (start us, length us, event | category | flops | bytes accessed | tf_op | source)
XLA Modules:
  0.0 94.7 jit_solution(8654843042355154446)
XLA Ops:
  0.0 0.0 copy-start.1
  0.0 10.3 %all_gather.12 = bf16[128,2048]{1,0:T(8,128)(2,1)S(1)} all-gather(bf16[64,2048]{1,0:T(8,128)(2,1)} %param.8), channel_id=1, replica_groups=mesh['sp'=16,'tp'=2] {'tp'}, dimensions={0}, use_global_device_ids=true | all-gather | bytes 786432 | tf_op jit(solution)/shard_map/all_gather | solution.py:19
  10.3 3.0 %fusion.28 = bf16[128,768]{0,1:T(8,128)(2,1)S(1)} fusion(bf16[128,2048]{1,0:T(8,128)(2,1)S(1)} %all_gather.12, bf16[2048,128]{1,0:T(8,128)(2,1)} %param.11, bf16[2048,128]{1,0:T(8,128)(2,1)} %param.10, bf16[2048,512]{1,0:T(8,128)(2,1)} %param.9), kind=kOutput, calls=%fused_computation.28 | convolution fusion | flops 412188672 | bytes 3866624 | tf_op jit(solution)/shard_map/dot_general | solution.py:18
  13.3 0.0 copy-done.1
  13.3 22.0 %all_gather.14 = f32[2048,8]{0,1:T(8,128)S(1)} all-gather(f32[128,8]{0,1:T(8,128)S(1)} %copy-done.1), channel_id=1, replica_groups=mesh['sp'=16,'tp'=2] {'sp'}, dimensions={0}, use_global_device_ids=true | all-gather | bytes 69632 | tf_op jit(solution)/shard_map/all_gather | solution.py:28
  35.3 0.0 copy-start
  35.4 18.9 %all_gather.15 = bf16[2048,128]{0,1:T(8,128)(2,1)S(1)} all-gather(bf16[128,128]{0,1:T(8,128)(2,1)S(1)} %get-tuple-element.118), channel_id=1, replica_groups=mesh['sp'=16,'tp'=2] {'sp'}, dimensions={0}, use_global_device_ids=true | all-gather | bytes 557056 | tf_op jit(solution)/shard_map/all_gather | solution.py:31
  54.3 20.3 %all_gather.13 = bf16[2048,128]{0,1:T(8,128)(2,1)S(1)} all-gather(bf16[128,128]{0,1:T(8,128)(2,1)S(1)} %get-tuple-element.119), channel_id=1, replica_groups=mesh['sp'=16,'tp'=2] {'sp'}, dimensions={0}, use_global_device_ids=true | all-gather | bytes 557056 | tf_op jit(solution)/shard_map/all_gather | solution.py:30
  74.6 0.0 copy-done
  74.6 9.0 %while.16 = (s32[]{:T(128)}, f32[128,2,4]{0,2,1:T(4,128)S(1)}, f32[128,2,4]{0,2,1:T(4,128)S(1)}, f32[128,2,4,64]{0,3,2,1:T(8,128)S(1)}, s32[]{:T(128)}, /*index=...) while((s32[]{:T(128)}, f32[128,2,4]{0,2,1:T(4,128)S(1)}, ...), condition=%wide.wide.region_3.4_spmd.clone, body=%wide.wide.region_0.3_spmd.clone.sunk | while | flops 577114240 | bytes 28210328 | solution.py:74
  74.6 0.3 broadcast_compare_fusion.3
  75.0 2.6 %fusion.57 = (f32[128,2,4]{0,2,1:T(4,128)S(1)}, f32[2,2048,128,4]{2,1,3,0:T(8,128)S(1)}) fusion(f32[2,4,2048]{2,1,0:T(4,128)S(1)} %bitcast.108, f32[128,2,4]{0,2,1:T(4,128)S(1)} %bitcast.120, pred[128,2048]{0,1:T(8,128)(4,1)S(1)} %broadcast_compare_fusion.3, bf16[2048,2,64,1]{0,2,3,1:T(8,128)(2,1)S(1)} %bitcast.114, ...), kind=kOutput, calls=%fused_computation.7.clone.clone.1 | convolution fusion | flops 278920192 | bytes 9379840 | tf_op jit(solution)/shard_map/while/body/tkgd,rkd->tkgr/dot_general | solution.py:47
  77.6 3.1 %fusion.58 = f32[128,2,4]{0,2,1:T(4,128)S(1)} fusion(f32[2,2048,128,4]{2,1,3,0:T(8,128)S(1)} %get-tuple-element.252, f32[128,2,4]{0,2,1:T(4,128)S(1)} %max.6, f32[2,4,2048]{2,1,0:T(4,128)S(1)} %bitcast.109, f32[128,2,4]{0,2,1:T(4,128)S(1)} %bitcast.121, pred[128,2048]{0,1:T(8,128)(4,1)S(1)} %broadcast_compare_fusion.3), kind=kLoop, calls=%fused_computation.6.clone.clone.1 | loop fusion | flops 14679040 | bytes 8728576 | tf_op jit(solution)/shard_map/while/body/reduce_sum | solution.py:60
  80.8 2.8 %fusion.59 = f32[128,2,4,64]{0,3,2,1:T(8,128)S(1)} fusion(bf16[2048,2,64,1]{0,2,3,1:T(8,128)(2,1)S(1)} %bitcast.113, f32[2,2048,128,4]{2,1,3,0:T(8,128)S(1)} %get-tuple-element.252, f32[128,2,4]{0,2,1:T(4,128)S(1)} %max.6, f32[2,4,2048]{2,1,0:T(4,128)S(1)} %bitcast.110, f32[128,2,4]{0,2,1:T(4,128)S(1)} %bitcast.122, ...), kind=kOutput, calls=%fused_computation.11.clone.clone.1 | convolution fusion | flops 283246592 | bytes 9777152 | tf_op jit(solution)/shard_map/while/body/tkgr,rkd->tkgd/dot_general | solution.py:61
  83.6 0.1 reshape.55
  83.8 0.1 copy.14
  83.9 7.0 %all_to_all.19 = bf16[2,64,512]{2,1,0:T(8,128)(2,1)S(1)} all-to-all(bf16[2,64,512]{2,1,0:T(8,128)(2,1)S(1)} %copy.14), channel_id=1, replica_groups=mesh['sp'=16,'tp'=2] {'tp'}, dimensions={0} | all-to-all | bytes 262144 | tf_op jit(solution)/shard_map/all_to_all | solution.py:76
  91.0 3.7 %convolution_convert_fusion = bf16[64,2048]{1,0:T(8,128)(2,1)} fusion(bf16[64,1024]{1,0:T(8,128)(2,1)S(1)} %bitcast.112, bf16[1024,2048]{1,0:T(8,128)(2,1)} %param.13), kind=kOutput, calls=%fused_computation.26 | convolution fusion | flops 268566528 | bytes 4587520 | tf_op jit(solution)/shard_map/dot_general | solution.py:77
  (13 shorter events, 0.1 us)
Async XLA Ops:
  0.0 13.3 %copy-start.1 = (f32[128,8]{0,1:T(8,128)S(1)}, f32[128,8]{0,1:T(8,128)}, u32[]{:S(2)}) copy-start(f32[128,8]{0,1:T(8,128)} %param.12) | copy-start | bytes 12292
  35.3 39.2 %copy-start = (f32[2048,8]{0,1:T(8,128)}, f32[2048,8]{0,1:T(8,128)S(1)}, u32[]{:S(2)}) copy-start(f32[2048,8]{0,1:T(8,128)S(1)} %all_gather.14) | copy-start | bytes 196612
where the time goes:
time: 94.9 us; the launch traced here: 94.7 us
  blocking collectives  78.5 us (83%)
  matrix products  12.1 us (13%)
  other arithmetic  3.53 us (4%)
    all_gather x1, blocking collectives, shards(): gate_every = lax.all_gather(cum_gate, 'sp', axis=0, tiled=True)  22 us
    all_gather x1, blocking collectives, shards(): lax.all_gather(keys, 'sp', axis=0, tiled=True)  20.3 us
    all_gather x1, blocking collectives, shards(): lax.all_gather(values, 'sp', axis=0, tiled=True)  18.9 us
    all_gather x1, blocking collectives, shards(): lax.all_gather(tokens, 'tp', axis=0, tiled=True)  10.3 us
    all_to_all x1, blocking collectives, shards(): lax.all_to_all(attended, 'tp', split_axis=0, concat_axis=1, tiled=True)  7.03 us
    dot_general x1, matrix products, shards(): jnp.dot(regrouped, w_out, preferred_element_type=jnp.float32)  3.74 us
    reduce_sum x1, other arithmetic, add_block(): new_total = run_total * factor + jnp.sum(weights, axis=-1)  3.13 us
    dot_general x1, matrix products, shards(): jnp.dot(lax.all_gather(tokens, 'tp', axis=0, tiled=True), stacked, prefer...  2.96 us

commit v1 on v0

--- a/solution.py
+++ b/solution.py
@@ -25,7 +25,18 @@
     keys = joined[:, query_cols : query_cols + pair_cols]
     values = joined[:, query_cols + pair_cols :]
     gate_query = cum_gate.reshape(row_count, local_kv, group)
-    gate_every = lax.all_gather(cum_gate, "sp", axis=0, tiled=True)
+    ledger = []
+    axis_total = lax.axis_size("sp")
+    for rr in [*range(1, axis_total)]:
+        ledger.append((rr - 1, rr))
+    known = cum_gate
+    local_now = ledger + [(axis_total - 1, 0)]
+    heap = [known]
+    for _ in tuple(range(axis_total - 1)):
+        known = lax.ppermute(known, axis_name="sp", perm=local_now)
+        heap += [known]
+    v_now = jnp.concatenate([*reversed(heap)], 0)
+    gate_every = jnp.roll(v_now, (lax.axis_index("sp") + 1) * known.shape[0], 0)
     keys_every, values_every = (
         lax.all_gather(keys, "sp", axis=0, tiled=True),
         lax.all_gather(values, "sp", axis=0, tiled=True),

time: 94.9 us -> 139 us (1.46)
  waiting for transfers between devices: 0 us -> 66.6 us
  blocking collectives: 78.5 us -> 54.4 us
    ppermute x0 -> x15, waiting for transfers between devices: none -> 66.6 us  [shards(): known = lax.ppermute(known, axis_name='sp', perm=local_now)]
    all_gather x1 -> x0, blocking collectives: 22 us -> none  [shards(): gate_every = lax.all_gather(cum_gate, 'sp', axis=0, tiled=True)]
    all_gather x1, blocking collectives: 10.3 us -> 7.24 us  [shards(): lax.all_gather(tokens, 'tp', axis=0, tiled=True)]
  transfers between devices with their start and end apart: 0 -> 15, of which waited for: 0 -> 12; matrix products, arithmetic and copies ran while one was open for 0% -> 2% of each run, Pallas kernels for 0% -> 0%
where the time goes in v1:
time: 139 us
  waiting for transfers between devices  66.6 us (48%)
  blocking collectives  54.4 us (39%)
  matrix products  12.1 us (9%)
  other arithmetic  3.53 us (3%)
    ppermute x15, waiting for transfers between devices, shards(): known = lax.ppermute(known, axis_name='sp', perm=local_now)  66.6 us
    all_gather x1, blocking collectives, shards(): lax.all_gather(keys, 'sp', axis=0, tiled=True)  20.4 us
    all_gather x1, blocking collectives, shards(): lax.all_gather(values, 'sp', axis=0, tiled=True)  19.4 us
    all_to_all x1, blocking collectives, shards(): lax.all_to_all(attended, 'tp', split_axis=0, concat_axis=1, tiled=True)  7.4 us
    all_gather x1, blocking collectives, shards(): lax.all_gather(tokens, 'tp', axis=0, tiled=True)  7.24 us
    dot_general x1, matrix products, shards(): jnp.dot(regrouped, w_out, preferred_element_type=jnp.float32)  3.74 us
    reduce_sum x1, other arithmetic, add_block(): new_total = run_total * factor + jnp.sum(weights, axis=-1)  3.13 us
    dot_general x1, matrix products, shards(): jnp.dot(lax.all_gather(tokens, 'tp', axis=0, tiled=True), stacked, prefer...  2.96 us
  transfers between devices with their start and end apart: 15, of which 12 were waited for; matrix products, arithmetic and copies ran while one was open for 2% of the time, Pallas kernels for 0%

profile of v1, /device:TPU:0, one launch (start us, length us, event | category | flops | bytes accessed | tf_op | source)
XLA Modules:
  0.0 138.8 jit_solution(2529899165938277782)
XLA Ops:
  0.0 0.5 collective-permute-start
  0.5 6.6 %collective-permute-done = f32[128,8]{0,1:T(8,128)S(1)} collective-permute-done((f32[128,8]{0,1:T(8,128)}, f32[128,8]{0,1:T(8,128)S(1)}, u32[]{:S(2)}, u32[]{:S(2)}) %collective-permute-start) | collective-permute-done | bytes 4128 | tf_op jit(solution)/shard_map/ppermute | solution.py:36
  7.0 0.0 collective-permute-start.1
  7.0 5.7 %collective-permute-done.1 = f32[128,8]{0,1:T(8,128)S(1)} collective-permute-done((f32[128,8]{0,1:T(8,128)S(1)}, f32[128,8]{0,1:T(8,128)S(1)}, u32[]{:S(2)}, u32[]{:S(2)}) %collective-permute-start.1) | collective-permute-done | bytes 4128 | tf_op jit(solution)/shard_map/ppermute | solution.py:36
  12.8 0.0 collective-permute-start.2
  12.8 5.7 %collective-permute-done.2 = f32[128,8]{0,1:T(8,128)S(1)} collective-permute-done((f32[128,8]{0,1:T(8,128)S(1)}, f32[128,8]{0,1:T(8,128)S(1)}, u32[]{:S(2)}, u32[]{:S(2)}) %collective-permute-start.2) | collective-permute-done | bytes 4128 | tf_op jit(solution)/shard_map/ppermute | solution.py:36
  18.5 0.0 collective-permute-start.3
  18.5 5.7 %collective-permute-done.3 = f32[128,8]{0,1:T(8,128)S(1)} collective-permute-done((f32[128,8]{0,1:T(8,128)S(1)}, f32[128,8]{0,1:T(8,128)S(1)}, u32[]{:S(2)}, u32[]{:S(2)}) %collective-permute-start.3) | collective-permute-done | bytes 4128 | tf_op jit(solution)/shard_map/ppermute | solution.py:36
  24.2 5.7 %collective-permute-done.4 = f32[128,8]{0,1:T(8,128)S(1)} collective-permute-done((f32[128,8]{0,1:T(8,128)S(1)}, f32[128,8]{0,1:T(8,128)S(1)}, u32[]{:S(2)}, u32[]{:S(2)}) %collective-permute-start.4) | collective-permute-done | bytes 4128 | tf_op jit(solution)/shard_map/ppermute | solution.py:36
  30.0 5.7 %collective-permute-done.5 = f32[128,8]{0,1:T(8,128)S(1)} collective-permute-done((f32[128,8]{0,1:T(8,128)S(1)}, f32[128,8]{0,1:T(8,128)S(1)}, u32[]{:S(2)}, u32[]{:S(2)}) %collective-permute-start.5) | collective-permute-done | bytes 4128 | tf_op jit(solution)/shard_map/ppermute | solution.py:36
  35.7 5.7 %collective-permute-done.6 = f32[128,8]{0,1:T(8,128)S(1)} collective-permute-done((f32[128,8]{0,1:T(8,128)S(1)}, f32[128,8]{0,1:T(8,128)S(1)}, u32[]{:S(2)}, u32[]{:S(2)}) %collective-permute-start.6) | collective-permute-done | bytes 4128 | tf_op jit(solution)/shard_map/ppermute | solution.py:36
  41.4 5.7 %collective-permute-done.7 = f32[128,8]{0,1:T(8,128)S(1)} collective-permute-done((f32[128,8]{0,1:T(8,128)S(1)}, f32[128,8]{0,1:T(8,128)S(1)}, u32[]{:S(2)}, u32[]{:S(2)}) %collective-permute-start.7) | collective-permute-done | bytes 4128 | tf_op jit(solution)/shard_map/ppermute | solution.py:36
  47.2 5.7 %collective-permute-done.8 = f32[128,8]{0,1:T(8,128)S(1)} collective-permute-done((f32[128,8]{0,1:T(8,128)S(1)}, f32[128,8]{0,1:T(8,128)S(1)}, u32[]{:S(2)}, u32[]{:S(2)}) %collective-permute-start.8) | collective-permute-done | bytes 4128 | tf_op jit(solution)/shard_map/ppermute | solution.py:36
  52.9 5.7 %collective-permute-done.9 = f32[128,8]{0,1:T(8,128)S(1)} collective-permute-done((f32[128,8]{0,1:T(8,128)S(1)}, f32[128,8]{0,1:T(8,128)S(1)}, u32[]{:S(2)}, u32[]{:S(2)}) %collective-permute-start.9) | collective-permute-done | bytes 4128 | tf_op jit(solution)/shard_map/ppermute | solution.py:36
  58.6 7.2 %all_gather.9 = bf16[128,2048]{1,0:T(8,128)(2,1)S(1)} all-gather(bf16[64,2048]{1,0:T(8,128)(2,1)} %param.8), channel_id=1, replica_groups=mesh['sp'=16,'tp'=2] {'tp'}, dimensions={0}, use_global_device_ids=true | all-gather | bytes 786432 | tf_op jit(solution)/shard_map/all_gather | solution.py:19
  65.9 3.0 %fusion.28 = bf16[128,768]{0,1:T(8,128)(2,1)S(1)} fusion(bf16[128,2048]{1,0:T(8,128)(2,1)S(1)} %all_gather.9, bf16[2048,128]{1,0:T(8,128)(2,1)} %param.11, bf16[2048,128]{1,0:T(8,128)(2,1)} %param.10, bf16[2048,512]{1,0:T(8,128)(2,1)} %param.9), kind=kOutput, calls=%fused_computation.28 | convolution fusion | flops 412188672 | bytes 3866624 | tf_op jit(solution)/shard_map/dot_general | solution.py:18
  68.8 2.8 %collective-permute-done.11 = f32[128,8]{0,1:T(8,128)S(1)} collective-permute-done((f32[128,8]{0,1:T(8,128)S(1)}, f32[128,8]{0,1:T(8,128)S(1)}, u32[]{:S(2)}, u32[]{:S(2)}) %collective-permute-start.11) | collective-permute-done | bytes 4128 | tf_op jit(solution)/shard_map/ppermute | solution.py:36
  71.6 5.7 %collective-permute-done.12 = f32[128,8]{0,1:T(8,128)S(1)} collective-permute-done((f32[128,8]{0,1:T(8,128)S(1)}, f32[128,8]{0,1:T(8,128)S(1)}, u32[]{:S(2)}, u32[]{:S(2)}) %collective-permute-start.12) | collective-permute-done | bytes 4128 | tf_op jit(solution)/shard_map/ppermute | solution.py:36
  77.3 19.4 %all_gather.11 = bf16[2048,128]{0,1:T(8,128)(2,1)S(1)} all-gather(bf16[128,128]{0,1:T(8,128)(2,1)S(1)} %get-tuple-element.118), channel_id=1, replica_groups=mesh['sp'=16,'tp'=2] {'sp'}, dimensions={0}, use_global_device_ids=true | all-gather | bytes 557056 | tf_op jit(solution)/shard_map/all_gather | solution.py:42
  96.8 0.2 collective-permute-start.14
  96.9 20.4 %all_gather.10 = bf16[2048,128]{0,1:T(8,128)(2,1)S(1)} all-gather(bf16[128,128]{0,1:T(8,128)(2,1)S(1)} %get-tuple-element.119), channel_id=1, replica_groups=mesh['sp'=16,'tp'=2] {'sp'}, dimensions={0}, use_global_device_ids=true | all-gather | bytes 557056 | tf_op jit(solution)/shard_map/all_gather | solution.py:41
  117.7 0.0 copy-start
  117.8 0.5 copy-done
  118.4 8.9 %while.16 = (s32[]{:T(128)}, f32[128,2,4]{0,2,1:T(4,128)S(1)}, f32[128,2,4]{0,2,1:T(4,128)S(1)}, f32[128,2,4,64]{0,3,2,1:T(8,128)S(1)}, s32[]{:T(128)}, /*index=...) while((s32[]{:T(128)}, f32[128,2,4]{0,2,1:T(4,128)S(1)}, ...), condition=%wide.wide.region_3.4_spmd.clone, body=%wide.wide.region_0.3_spmd.clone.sunk | while | flops 577114240 | bytes 28210328 | solution.py:85
  118.4 0.3 broadcast_compare_fusion.3
  118.7 2.6 %fusion.57 = (f32[128,2,4]{0,2,1:T(4,128)S(1)}, f32[2,2048,128,4]{2,1,3,0:T(8,128)S(1)}) fusion(f32[2,4,2048]{2,1,0:T(4,128)S(1)} %bitcast.108, f32[128,2,4]{0,2,1:T(4,128)S(1)} %bitcast.118, pred[128,2048]{0,1:T(8,128)(4,1)S(1)} %broadcast_compare_fusion.3, bf16[2048,2,64,1]{0,2,3,1:T(8,128)(2,1)S(1)} %bitcast.114, ...), kind=kOutput, calls=%fused_computation.7.clone.clone.1 | convolution fusion | flops 278920192 | bytes 9379840 | tf_op jit(solution)/shard_map/while/body/tkgd,rkd->tkgr/dot_general | solution.py:58
  121.3 3.1 %fusion.58 = f32[128,2,4]{0,2,1:T(4,128)S(1)} fusion(f32[2,2048,128,4]{2,1,3,0:T(8,128)S(1)} %get-tuple-element.252, f32[128,2,4]{0,2,1:T(4,128)S(1)} %max.6, f32[2,4,2048]{2,1,0:T(4,128)S(1)} %bitcast.109, f32[128,2,4]{0,2,1:T(4,128)S(1)} %bitcast.119, pred[128,2048]{0,1:T(8,128)(4,1)S(1)} %broadcast_compare_fusion.3), kind=kLoop, calls=%fused_computation.6.clone.clone.1 | loop fusion | flops 14679040 | bytes 8728576 | tf_op jit(solution)/shard_map/while/body/reduce_sum | solution.py:71
  124.5 2.8 %fusion.59 = f32[128,2,4,64]{0,3,2,1:T(8,128)S(1)} fusion(bf16[2048,2,64,1]{0,2,3,1:T(8,128)(2,1)S(1)} %bitcast.113, f32[2,2048,128,4]{2,1,3,0:T(8,128)S(1)} %get-tuple-element.252, f32[128,2,4]{0,2,1:T(4,128)S(1)} %max.6, f32[2,4,2048]{2,1,0:T(4,128)S(1)} %bitcast.110, f32[128,2,4]{0,2,1:T(4,128)S(1)} %bitcast.120, ...), kind=kOutput, calls=%fused_computation.11.clone.clone.1 | convolution fusion | flops 283246592 | bytes 9777152 | tf_op jit(solution)/shard_map/while/body/tkgr,rkd->tkgd/dot_general | solution.py:72
  127.3 0.1 reshape.55
  127.5 0.1 copy.14
  127.6 7.4 %all_to_all.19 = bf16[2,64,512]{2,1,0:T(8,128)(2,1)S(1)} all-to-all(bf16[2,64,512]{2,1,0:T(8,128)(2,1)S(1)} %copy.14), channel_id=1, replica_groups=mesh['sp'=16,'tp'=2] {'tp'}, dimensions={0} | all-to-all | bytes 262144 | tf_op jit(solution)/shard_map/all_to_all | solution.py:87
  135.1 3.7 %convolution_convert_fusion = bf16[64,2048]{1,0:T(8,128)(2,1)} fusion(bf16[64,1024]{1,0:T(8,128)(2,1)S(1)} %bitcast.112, bf16[1024,2048]{1,0:T(8,128)(2,1)} %param.13), kind=kOutput, calls=%fused_computation.26 | convolution fusion | flops 268566528 | bytes 4587520 | tf_op jit(solution)/shard_map/dot_general | solution.py:88
  (61 shorter events, 0.3 us)
Async XLA Ops:
  0.0 117.5 %copy-start.1 = (f32[128,8]{0,1:T(8,128)S(1)}, f32[128,8]{0,1:T(8,128)}, u32[]{:S(2)}) copy-start(f32[128,8]{0,1:T(8,128)} %param.12) | copy-start | bytes 12292
  0.0 7.0 %collective-permute-start = (f32[128,8]{0,1:T(8,128)}, f32[128,8]{0,1:T(8,128)S(1)}, u32[]{:S(2)}, u32[]{:S(2)}) collective-permute-start(f32[128,8]{0,1:T(8,128)} %param.12), channel_id=1, source_target_pairs={{0,2},{2,4},{4,6},{6,8},{8,10},{10,12},{12,14},{14,16},{16,18},{18... | collective-permute-start | bytes 12296 | tf_op jit(solution)/shard_map/ppermute | solution.py:36
  7.0 5.7 %collective-permute-start.1 = (f32[128,8]{0,1:T(8,128)S(1)}, f32[128,8]{0,1:T(8,128)S(1)}, u32[]{:S(2)}, u32[]{:S(2)}) collective-permute-start(f32[128,8]{0,1:T(8,128)S(1)} %collective-permute-done), channel_id=1, source_target_pairs={{0,2},{2,4},{4,6},{6,8},{8,10},{10,12},{12,14},{14,16},{16,18},{18... | collective-permute-start | bytes 12296 | tf_op jit(solution)/shard_map/ppermute | solution.py:36
  12.8 5.7 %collective-permute-start.2 = (f32[128,8]{0,1:T(8,128)S(1)}, f32[128,8]{0,1:T(8,128)S(1)}, u32[]{:S(2)}, u32[]{:S(2)}) collective-permute-start(f32[128,8]{0,1:T(8,128)S(1)} %collective-permute-done.1), channel_id=1, source_target_pairs={{0,2},{2,4},{4,6},{6,8},{8,10},{10,12},{12,14},{14,16},{16,18},{18... | collective-permute-start | bytes 12296 | tf_op jit(solution)/shard_map/ppermute | solution.py:36
  18.5 5.7 %collective-permute-start.3 = (f32[128,8]{0,1:T(8,128)S(1)}, f32[128,8]{0,1:T(8,128)S(1)}, u32[]{:S(2)}, u32[]{:S(2)}) collective-permute-start(f32[128,8]{0,1:T(8,128)S(1)} %collective-permute-done.2), channel_id=1, source_target_pairs={{0,2},{2,4},{4,6},{6,8},{8,10},{10,12},{12,14},{14,16},{16,18},{18... | collective-permute-start | bytes 12296 | tf_op jit(solution)/shard_map/ppermute | solution.py:36
  24.2 5.7 %collective-permute-start.4 = (f32[128,8]{0,1:T(8,128)S(1)}, f32[128,8]{0,1:T(8,128)S(1)}, u32[]{:S(2)}, u32[]{:S(2)}) collective-permute-start(f32[128,8]{0,1:T(8,128)S(1)} %collective-permute-done.3), channel_id=1, source_target_pairs={{0,2},{2,4},{4,6},{6,8},{8,10},{10,12},{12,14},{14,16},{16,18},{18... | collective-permute-start | bytes 12296 | tf_op jit(solution)/shard_map/ppermute | solution.py:36
  30.0 5.7 %collective-permute-start.5 = (f32[128,8]{0,1:T(8,128)S(1)}, f32[128,8]{0,1:T(8,128)S(1)}, u32[]{:S(2)}, u32[]{:S(2)}) collective-permute-start(f32[128,8]{0,1:T(8,128)S(1)} %collective-permute-done.4), channel_id=1, source_target_pairs={{0,2},{2,4},{4,6},{6,8},{8,10},{10,12},{12,14},{14,16},{16,18},{18... | collective-permute-start | bytes 12296 | tf_op jit(solution)/shard_map/ppermute | solution.py:36
  35.7 5.7 %collective-permute-start.6 = (f32[128,8]{0,1:T(8,128)S(1)}, f32[128,8]{0,1:T(8,128)S(1)}, u32[]{:S(2)}, u32[]{:S(2)}) collective-permute-start(f32[128,8]{0,1:T(8,128)S(1)} %collective-permute-done.5), channel_id=1, source_target_pairs={{0,2},{2,4},{4,6},{6,8},{8,10},{10,12},{12,14},{14,16},{16,18},{18... | collective-permute-start | bytes 12296 | tf_op jit(solution)/shard_map/ppermute | solution.py:36
  41.4 5.7 %collective-permute-start.7 = (f32[128,8]{0,1:T(8,128)S(1)}, f32[128,8]{0,1:T(8,128)S(1)}, u32[]{:S(2)}, u32[]{:S(2)}) collective-permute-start(f32[128,8]{0,1:T(8,128)S(1)} %collective-permute-done.6), channel_id=1, source_target_pairs={{0,2},{2,4},{4,6},{6,8},{8,10},{10,12},{12,14},{14,16},{16,18},{18... | collective-permute-start | bytes 12296 | tf_op jit(solution)/shard_map/ppermute | solution.py:36
  47.2 5.7 %collective-permute-start.8 = (f32[128,8]{0,1:T(8,128)S(1)}, f32[128,8]{0,1:T(8,128)S(1)}, u32[]{:S(2)}, u32[]{:S(2)}) collective-permute-start(f32[128,8]{0,1:T(8,128)S(1)} %collective-permute-done.7), channel_id=1, source_target_pairs={{0,2},{2,4},{4,6},{6,8},{8,10},{10,12},{12,14},{14,16},{16,18},{18... | collective-permute-start | bytes 12296 | tf_op jit(solution)/shard_map/ppermute | solution.py:36
  52.9 5.7 %collective-permute-start.9 = (f32[128,8]{0,1:T(8,128)S(1)}, f32[128,8]{0,1:T(8,128)S(1)}, u32[]{:S(2)}, u32[]{:S(2)}) collective-permute-start(f32[128,8]{0,1:T(8,128)S(1)} %collective-permute-done.8), channel_id=1, source_target_pairs={{0,2},{2,4},{4,6},{6,8},{8,10},{10,12},{12,14},{14,16},{16,18},{18... | collective-permute-start | bytes 12296 | tf_op jit(solution)/shard_map/ppermute | solution.py:36
  58.6 7.2 %collective-permute-start.10 = (f32[128,8]{0,1:T(8,128)S(1)}, f32[128,8]{0,1:T(8,128)S(1)}, u32[]{:S(2)}, u32[]{:S(2)}) collective-permute-start(f32[128,8]{0,1:T(8,128)S(1)} %collective-permute-done.9), channel_id=1, source_target_pairs={{0,2},{2,4},{4,6},{6,8},{8,10},{10,12},{12,14},{14,16},{16,18},{18... | collective-permute-start | bytes 12296 | tf_op jit(solution)/shard_map/ppermute | solution.py:36
  65.9 5.7 %collective-permute-start.11 = (f32[128,8]{0,1:T(8,128)S(1)}, f32[128,8]{0,1:T(8,128)S(1)}, u32[]{:S(2)}, u32[]{:S(2)}) collective-permute-start(f32[128,8]{0,1:T(8,128)S(1)} %collective-permute-done.10), channel_id=1, source_target_pairs={{0,2},{2,4},{4,6},{6,8},{8,10},{10,12},{12,14},{14,16},{16,18},{18... | collective-permute-start | bytes 12296 | tf_op jit(solution)/shard_map/ppermute | solution.py:36
  71.6 5.7 %collective-permute-start.12 = (f32[128,8]{0,1:T(8,128)S(1)}, f32[128,8]{0,1:T(8,128)S(1)}, u32[]{:S(2)}, u32[]{:S(2)}) collective-permute-start(f32[128,8]{0,1:T(8,128)S(1)} %collective-permute-done.11), channel_id=1, source_target_pairs={{0,2},{2,4},{4,6},{6,8},{8,10},{10,12},{12,14},{14,16},{16,18},{18... | collective-permute-start | bytes 12296 | tf_op jit(solution)/shard_map/ppermute | solution.py:36
  77.3 19.4 %collective-permute-start.13 = (f32[128,8]{0,1:T(8,128)S(1)}, f32[128,8]{0,1:T(8,128)S(1)}, u32[]{:S(2)}, u32[]{:S(2)}) collective-permute-start(f32[128,8]{0,1:T(8,128)S(1)} %collective-permute-done.12), channel_id=1, source_target_pairs={{0,2},{2,4},{4,6},{6,8},{8,10},{10,12},{12,14},{14,16},{16,18},{18... | collective-permute-start | bytes 12296 | tf_op jit(solution)/shard_map/ppermute | solution.py:36
  96.8 20.6 %collective-permute-start.14 = (f32[128,8]{0,1:T(8,128)S(1)}, f32[128,8]{0,1:T(8,128)S(1)}, u32[]{:S(2)}, u32[]{:S(2)}) collective-permute-start(f32[128,8]{0,1:T(8,128)S(1)} %collective-permute-done.13), channel_id=1, source_target_pairs={{0,2},{2,4},{4,6},{6,8},{8,10},{10,12},{12,14},{14,16},{16,18},{18... | collective-permute-start | bytes 12296 | tf_op jit(solution)/shard_map/ppermute | solution.py:36
  117.7 0.6 copy-start
